TPU v7x, 32 devices: a whole 2x2x4 slice. The times are simulated.
32 devices in a mesh: sp: 8 (over z, x), tp: 4 (over y, core).
Axes of the slice: x: 2, y: 2, z: 4, core: 2. Of those that a mesh axis runs over, the one named last changes fastest.
Arguments:
- stream: bfloat16 [2048, 2048], P('sp'), may hold values from -6 to 6
- query: bfloat16 [2048, 1024], P('sp', 'tp'), may hold values from -6 to 6
- forget_gate_logits: bfloat16 [2048, 1024], P('sp', 'tp'), may hold values from -4 to 4
- value_input_rows: bfloat16 [2048, 1024], P('sp', 'tp'), may hold values from -6 to 6
- output_gate_logits: bfloat16 [2048, 1024], P('sp', 'tp'), may hold values from -6 to 6
- forget_floor_margin: float32 [8, 128], P('tp'), as said below
- additional_fading_speed: float32 [2048, 8], P('sp', 'tp'), may hold values from -0.7 to 0, as said below
- head_norm_gain: float32 [128], replicated, may hold values from 0.1 to 1.9
- output_head_weight: bfloat16 [1024, 2048], replicated, may hold values from -0.1875 to 0.1875
- feedforward_norm_gain: float32 [2048], replicated, may hold values from 0.1 to 1.9
- selected_expert_index: int32 [2048, 2], P('sp'), may hold values from 0 to 7, all different within a row; in each aligned block of 64 rows (0 to 63, 64 to 127, ...) at most 32 rows name the same one
- selected_expert_weight: float32 [2048, 2], P(('sp', 'tp')), may hold values from 0.2 to 1
- expert_gate_weight: bfloat16 [8, 2048, 1024], P('sp', None, 'tp'), may hold values from -0.125 to 0.125
- expert_up_weight: bfloat16 [8, 2048, 1024], P('sp', None, 'tp'), may hold values from -0.125 to 0.125
- expert_down_weight: bfloat16 [8, 1024, 2048], P('sp', 'tp'), may hold values from -0.1875 to 0.1875
Outputs:
- layer_out: bfloat16 [2048, 2048], P(('sp', 'tp'))
Inputs may be any that keep to these rules, and one draw needn't show every extreme that they name: `forget_floor_margin`: positive. `additional_fading_speed`: zero at most positions. `selected_expert_index`: the 2 experts of a position differ; in each aligned block of 64 positions no expert is named more than 32 times, and in every draw some expert is named exactly 32 times in some block.
All inputs are finite; a program needn't handle non-finite values.
Results may differ from a plain program's by a relative error of at most 0.006.
Values may be sent and summed in bfloat16 or wider, within the bound.
A program may use at most 64 MiB of HBM per device.

v0:
```python
import jax
import jax.numpy as jnp
from jax import lax
from jax.sharding import PartitionSpec as P

BLOCK = 64


EPS = 1e-06
HIGH = lax.Precision.HIGHEST


def entering(part, axis, combine, identity):
    place = lax.axis_index(axis)
    gathered = jax.tree.map(lambda a: lax.all_gather(a, axis), part)
    state = jax.tree.map(lambda a, e: jnp.zeros_like(a) + jnp.asarray(e, a.dtype), part, identity)

    def one(turn, state):
        return combine(
            state, jax.tree.map(lambda a: lax.dynamic_index_in_dim(a, turn, 0, False), gathered)
        )

    return lax.fori_loop(0, place, one, state)


def cut_to_segments(array, segment_span, heads):
    width = array.shape[1] // heads
    shaped = array.astype(jnp.float32).reshape(
        array.shape[0] // segment_span, segment_span, heads, width
    )
    return jnp.transpose(shaped, (0, 2, 1, 3))


def slot_ranks(chosen, experts):
    onehot = (chosen[:, :, None] == jnp.arange(experts, dtype=jnp.int32)[None, None, :]).astype(
        jnp.int32
    )
    earlier = jnp.cumsum(onehot, axis=1) - onehot
    return jnp.sum(earlier * onehot, axis=2)


def expert_hidden(rows, w_gate, w_up):
    flat = rows.reshape(-1, rows.shape[-1])
    gate_part = jnp.dot(flat, w_gate, preferred_element_type=jnp.float32)
    up_part = jnp.dot(flat, w_up, preferred_element_type=jnp.float32)
    hidden = (jax.nn.silu(gate_part) * up_part).astype(jnp.bfloat16)
    return hidden.reshape(rows.shape[:-1] + (w_gate.shape[1],))


def chain_combine(earlier, later):
    return (earlier[0] * later[0], later[0][..., None] * earlier[1] + later[1])


def carry_step(state, pieces):
    return (jnp.exp(pieces[1])[..., None] * state + pieces[0], state)


def per_device(
    stream,
    query,
    forget_gate_logits,
    value_input_rows,
    output_gate_logits,
    forget_floor_margin,
    additional_fading_speed,
    head_norm_gain,
    output_head_weight,
    feedforward_norm_gain,
    selected_expert_index,
    selected_expert_weight,
    expert_gate_weight,
    expert_up_weight,
    expert_down_weight,
):
    f32 = jnp.float32
    tok_rows, model_width = stream.shape
    local_scan_lanes, head_dim = forget_floor_margin.shape
    segment_span = BLOCK
    tp_count = lax.axis_size("tp")
    tp_rank = lax.axis_index("tp")
    query_blk = cut_to_segments(query, segment_span, local_scan_lanes)
    scores_segment_slice = cut_to_segments(forget_gate_logits, segment_span, local_scan_lanes)
    value_blk = cut_to_segments(value_input_rows, segment_span, local_scan_lanes)
    spike_segment_slice = cut_to_segments(additional_fading_speed, segment_span, local_scan_lanes)
    clearance_amount = forget_floor_margin[None, :, None, :]
    logarithmic_fading_speed = (
        jnp.logaddexp(
            jnp.log1p(-clearance_amount),
            jnp.log(clearance_amount) + jax.nn.log_sigmoid(scores_segment_slice),
        )
        + spike_segment_slice
    )
    key_in = clearance_amount * jax.nn.sigmoid(-scores_segment_slice)
    cumul = jnp.cumsum(logarithmic_fading_speed, axis=2)
    last = cumul[:, :, -1:, :]
    causal = jnp.tril(jnp.ones((segment_span, segment_span), dtype=bool))[:, :, None]
    pair_log = cumul[:, :, :, None, :] - cumul[:, :, None, :, :]
    decay = jnp.exp(jnp.where(causal, pair_log, -jnp.inf))
    scores = jnp.sum(query_blk[:, :, :, None, :] * key_in[:, :, None, :, :] * decay, axis=-1)
    inner = jnp.einsum("bhts,bhse->bhte", scores, value_blk, precision=HIGH)
    block_state = jnp.einsum(
        "bhsd,bhse->bhde", key_in * jnp.exp(last - cumul), value_blk, precision=HIGH
    )
    block_last = last[:, :, 0, :]
    last_cumul = jnp.cumsum(block_last, axis=0)
    device_decay = jnp.exp(last_cumul[-1])
    zero_state = jnp.zeros(block_state.shape[1:], f32)
    suffix = jnp.exp(last_cumul[-1][None] - last_cumul)
    local_final = jnp.sum(suffix[..., None] * block_state, axis=0)
    carried = entering(
        (device_decay, local_final), "sp", chain_combine, (jnp.ones_like(device_decay), zero_state)
    )
    incoming = carried[1]
    _, chain_starts = lax.scan(carry_step, incoming, (block_state, block_last))
    recur = inner + jnp.einsum(
        "bhtd,bhde->bhte", query_blk * jnp.exp(cumul), chain_starts, precision=HIGH
    )
    recur = jnp.transpose(recur, (0, 2, 1, 3)).reshape(tok_rows, local_scan_lanes, head_dim)
    scale = lax.rsqrt(jnp.mean(recur * recur, axis=-1, keepdims=True) + EPS)
    gate_in = output_gate_logits.astype(f32).reshape(tok_rows, local_scan_lanes, head_dim)
    gated = (
        (recur * scale * head_norm_gain * jax.nn.silu(gate_in))
        .astype(jnp.bfloat16)
        .reshape(tok_rows, local_scan_lanes * head_dim)
    )
    projected = jnp.dot(
        lax.all_gather(gated, "tp", axis=1, tiled=True),
        output_head_weight,
        preferred_element_type=f32,
    )
    mixed = (stream.astype(f32) + projected).astype(jnp.bfloat16)
    mixed_wide = lax.optimization_barrier(mixed).astype(f32)
    normed = (
        mixed_wide
        * lax.rsqrt(jnp.mean(mixed_wide * mixed_wide, axis=-1, keepdims=True) + EPS)
        * feedforward_norm_gain
    ).astype(jnp.bfloat16)
    topk = selected_expert_index.shape[1]
    experts = lax.axis_size("sp") * expert_gate_weight.shape[0]
    group_rows = tok_rows // tp_count
    cap = 2 * topk * group_rows // experts
    assigned = group_rows * topk
    w_gate = expert_gate_weight[0]
    w_up = expert_up_weight[0]
    w_down = expert_down_weight[0]
    own_route = lax.dynamic_slice_in_dim(selected_expert_index, tp_rank * group_rows, group_rows, 0)
    own_ranks = slot_ranks(own_route.reshape(1, -1), experts)[0]
    padded = jnp.concatenate([normed, jnp.zeros((1, model_width), jnp.bfloat16)], axis=0)
    dest = own_route.reshape(-1) * cap + own_ranks
    owner = tp_rank * group_rows + jnp.arange(assigned, dtype=jnp.int32) // topk
    table = jnp.full((experts * cap,), tok_rows, jnp.int32).at[dest].set(owner)
    outgoing = padded[table].reshape(1, experts, cap, model_width)
    arrived = lax.all_to_all(outgoing, "sp", split_axis=1, concat_axis=1, tiled=True)
    hidden = expert_hidden(lax.all_gather(arrived, "tp", axis=0, tiled=True), w_gate, w_up)
    hidden_flat = hidden.reshape(-1, hidden.shape[-1])
    summed = lax.psum_scatter(
        jnp.dot(hidden_flat, w_down, preferred_element_type=f32),
        "tp",
        scatter_dimension=0,
        tiled=True,
    )
    expert_out = summed.astype(jnp.bfloat16).reshape(experts, cap, model_width)
    returned = lax.all_to_all(expert_out, "sp", split_axis=0, concat_axis=0, tiled=True)
    index = own_route.reshape(-1) * cap + own_ranks
    picked = (
        returned.reshape(-1, model_width)[index].astype(f32).reshape(group_rows, topk, model_width)
    )
    routed = jnp.sum(picked * selected_expert_weight[:, :, None], axis=1)
    own_mixed = lax.dynamic_slice_in_dim(mixed_wide, tp_rank * group_rows, group_rows, 0)
    return (own_mixed + routed).astype(jnp.bfloat16)


def solution(mesh):
    return jax.shard_map(
        per_device,
        mesh=mesh,
        in_specs=(
            P("sp", None),
            P("sp", "tp"),
            P("sp", "tp"),
            P("sp", "tp"),
            P("sp", "tp"),
            P("tp", None),
            P("sp", "tp"),
            P(),
            P(),
            P(),
            P("sp", None),
            P(("sp", "tp"), None),
            P("sp", None, "tp"),
            P("sp", None, "tp"),
            P("sp", "tp", None),
        ),
        out_specs=P(("sp", "tp"), None),
        check_vma=False,
    )
```

profile of v0, /device:TPU:8, one launch (start us, length us, event | category | flops | bytes accessed | tf_op | source)
XLA Modules:
  0.0 273.9 jit_solution(6115730861671469166)
XLA Ops:
  6.5 1.1 fusion.16
  7.6 0.1 neg.39
  7.8 0.7 negate_log-plus-one_fusion
  8.5 0.8 reshape.215
  9.2 0.3 select_add_fusion
  9.6 0.2 reduce_window_sum.33
  9.8 0.1 div.35
  10.0 1.0 reshape.223
  11.0 0.9 reshape.216
  12.0 0.7 fusion.28
  12.7 1.3 multiply_reduce_fusion.3
  14.1 0.0 all-gather.6.cloned.1.call-update
  14.1 0.0 all-gather.4.cloned.1.call-start
  14.2 0.1 broadcast_multiply_fusion
  14.2 0.1 copy.77
  14.3 0.1 eq.27
  14.5 0.1 fusion.42
  14.6 0.2 reduce_window_sum.35
  14.7 0.2 select_reduce_fusion
  14.9 0.1 copy.76
  15.0 0.1 mul.185
  15.2 1.0 scatter_custom_fusion
  16.2 18.0 %all_gather.16 = f32[8,2,128]{2,1,0:T(2,128)S(1)} all-gather(f32[1,2,128]{2,1,0:T(2,128)S(1)} %get-tuple-element.103), channel_id=1, replica_groups=mesh['sp'=8,'tp'=4] {'sp'}, dimensions={0}, use_global_device_ids=true | all-gather | bytes 9216 | tf_op jit(solution)/shard_map/all_gather | solution.py:15
  34.2 5.5 %multiply_reduce_fusion = f32[4,2,64,64]{3,2,1,0:T(8,128)S(1)} fusion(f32[4,2,64,128]{3,2,1,0:T(8,128)S(1)} %reduce_window_sum.33, f32[4,2,64,128]{3,2,1,0:T(8,128)S(1)} %get-tuple-element.110, f32[4,2,64,128]{3,2,1,0:T(8,128)S(1)} %get-tuple-element.111, pred[64,64]{1,0:T(8,128)(4,1)S(1)} %iota_compare_fusion.1), kind=kLoop, calls=%fused_computation.8 | loop fusion | flops 20938752 | bytes 921600 | tf_op jit(solution)/shard_map/reduce_sum | solution.py:99
  39.7 0.3 fusion.37
  40.0 0.0 copy-start.2
  40.0 14.5 %all-gather.6.cloned.1.call-done = f32[16,128,128]{2,1,0:T(8,128)} async-done(((f32[2,128,128]{2,1,0:T(8,128)}), f32[16,128,128]{2,1,0:T(8,128)}) %all-gather.6.cloned.1.call-update) | async-done | bytes 1048592 | tf_op jit(solution)/shard_map/all_gather | solution.py:15
  54.5 2.2 while.24
  54.6 1.0 bitcast_add_fusion.5
  55.6 1.0 bitcast_add_fusion.5
  56.7 0.7 while.25
  56.7 0.1 bitcast_add_fusion.6
  56.9 0.1 bitcast_add_fusion.6
  57.1 0.1 bitcast_add_fusion.6
  57.3 0.1 bitcast_add_fusion.6
  57.4 0.7 multiply_reduce_fusion.4
  58.1 0.1 copy.81
  58.3 0.2 copy.73
  58.5 0.3 mul.169
  58.8 0.1 fusion.35
  58.9 7.2 %all_gather.19 = bf16[256,1024]{1,0:T(8,128)(2,1)S(1)} all-gather(bf16[256,256]{1,0:T(8,128)(2,1)S(1)} %fusion.35), channel_id=1, replica_groups=mesh['sp'=8,'tp'=4] {'tp'}, dimensions={1}, use_global_device_ids=true | all-gather | bytes 655360 | tf_op jit(solution)/shard_map/all_gather | solution.py:127
  66.1 3.8 %fusion = bf16[256,2048]{1,0:T(8,128)(2,1)S(1)} fusion(bf16[256,1024]{1,0:T(8,128)(2,1)S(1)} %all_gather.19, bf16[1024,2048]{1,0:T(8,128)(2,1)} %param.27, bf16[256,2048]{1,0:T(8,128)(2,1)} %param.19), kind=kOutput, calls=%fused_computation.10 | convolution fusion | flops 1075314688 | bytes 6815744 | tf_op jit(solution)/shard_map/dot_general | solution.py:126
  69.9 0.3 multiply_reduce_fusion.1
  70.2 0.3 multiply_convert_fusion
  70.5 0.1 concatenate.3
  70.6 2.4 gather_fusion
  73.0 35.8 %all_to_all.10 = bf16[1,8,32,2048]{3,2,0,1:T(8,128)(2,1)} all-to-all(bf16[1,8,32,2048]{3,2,0,1:T(8,128)(2,1)} %bitcast.118), channel_id=1, replica_groups=mesh['sp'=8,'tp'=4] {'sp'}, dimensions={1} | all-to-all | bytes 2097152 | tf_op jit(solution)/shard_map/all_to_all | solution.py:153
  108.7 0.0 all-gather.4.cloned.1.call-update
  108.8 0.2 reduce-scatter.2.cloned.1.call-start
  109.0 33.1 %all-gather.4.cloned.1.call-done = bf16[4,8,32,2048]{3,2,1,0:T(8,128)(2,1)} async-done(((bf16[1,8,32,2048]{3,2,1,0:T(8,128)(2,1)}), bf16[4,8,32,2048]{3,2,1,0:T(8,128)(2,1)}) %all-gather.4.cloned.1.call-update) | async-done | bytes 4194320 | tf_op jit(solution)/shard_map/all_gather | solution.py:154
  142.1 4.8 %fusion.7 = f32[1024,256]{1,0:T(8,128)} fusion(bf16[1024,2048]{1,0:T(8,128)(2,1)} %bitcast.120, bf16[1,2048,256]{2,1,0:T(8,128)(2,1)} %param.31), kind=kOutput, calls=%fused_computation.20 | convolution fusion | flops 1073741824 | bytes 6291456 | tf_op jit(solution)/shard_map/dot_general | solution.py:44
  146.9 10.0 %fusion.2 = f32[1024,2048]{1,0:T(8,128)} fusion(bf16[1024,2048]{1,0:T(8,128)(2,1)} %bitcast.121, bf16[1,256,2048]{2,1,0:T(8,128)(2,1)S(1)} %copy-done, bf16[1,2048,256]{2,1,0:T(8,128)(2,1)S(1)} %copy-done.1, f32[1024,256]{1,0:T(8,128)} %fusion.7), kind=kOutput, calls=%fused_computation.15 | convolution fusion | flops 2149056512 | bytes 15728640 | tf_op jit(solution)/shard_map/dot_general | solution.py:157
  157.0 0.0 reduce-scatter.2.cloned.1.call-update
  157.0 0.0 copy-start.4
  157.0 71.5 %reduce-scatter.2.cloned.1.call-done = f32[256,2048]{1,0:T(8,128)} async-done(((f32[1024,2048]{1,0:T(8,128)}), f32[256,2048]{1,0:T(8,128)}) %reduce-scatter.2.cloned.1.call-update) | async-done | bytes 2097168 | tf_op jit(solution)/shard_map/reduce_scatter | solution.py:156
  228.6 2.7 convert_element_type.64
  231.3 6.0 %all-to-all-start.1 = ((bf16[8,32,2048]{2,1,0:T(8,128)(2,1)}), bf16[8,32,2048]{2,1,0:T(8,128)(2,1)S(1)}, u32[]{:S(2)}, u32[]{:S(2)}) async-start(bf16[8,32,2048]{2,1,0:T(8,128)(2,1)} %bitcast.117), calls=%async_computation.2 | async-start | bytes 2097152 | tf_op jit(solution)/shard_map/all_to_all | solution.py:163
  237.3 0.1 copy.80
  237.4 1.6 convert_element_type.60
  239.0 21.5 %all-to-all-done.1 = bf16[8,32,2048]{2,1,0:T(8,128)(2,1)S(1)} async-done(((bf16[8,32,2048]{2,1,0:T(8,128)(2,1)}), bf16[8,32,2048]{2,1,0:T(8,128)(2,1)S(1)}, u32[]{:S(2)}, u32[]{:S(2)}) %all-to-all-start.1) | async-done | bytes 1048608 | tf_op jit(solution)/shard_map/all_to_all | solution.py:163
  260.5 1.7 gather_fusion.1
  262.3 1.7 reshape.222
  264.0 1.5 multiply_reduce_fusion.2
  265.5 1.8 add_convert_fusion
  (40 shorter events, 0.2 us)
Async XLA Ops:
  6.5 140.4 %copy-start = (bf16[1,256,2048]{2,1,0:T(8,128)(2,1)S(1)}, bf16[1,256,2048]{2,1,0:T(8,128)(2,1)}, u32[]{:S(2)}) copy-start(bf16[1,256,2048]{2,1,0:T(8,128)(2,1)} %param.33) | copy-start | bytes 3145732
  6.5 7.6 %copy-start.5 = (s32[256,2]{0,1:T(2,128)S(1)}, s32[256,2]{0,1:T(2,128)}, u32[]{:S(2)}) copy-start(s32[256,2]{0,1:T(2,128)} %param.29) | copy-start | bytes 6148
  6.5 27.7 %copy-start.6 = (f32[128]{0:T(128)S(1)}, f32[128]{0:T(128)}, u32[]{:S(2)}) copy-start(f32[128]{0:T(128)} %param.26) | copy-start | bytes 1540
  6.5 48.0 %all-gather.6.cloned.1.call-start = ((), (), s32[]{:S(2)}) async-start(), calls=%async_computation.5 | async-start | bytes 1179648 | tf_op jit(solution)/shard_map/all_gather | solution.py:15
  14.1 128.1 %all-gather.4.cloned.1.call-start = ((), (), s32[]{:S(2)}) async-start(), calls=%async_computation.3 | async-start | bytes 5242880 | tf_op jit(solution)/shard_map/all_gather | solution.py:154
  40.0 18.8 %copy-start.2 = (bf16[256,256]{1,0:T(8,128)(2,1)S(1)}, bf16[256,256]{1,0:T(8,128)(2,1)}, u32[]{:S(2)}) copy-start(bf16[256,256]{1,0:T(8,128)(2,1)} %param.23) | copy-start | bytes 393220
  66.1 4.1 %copy-start.3 = (f32[2048]{0:T(1024)S(1)}, f32[2048]{0:T(1024)}, u32[]{:S(2)}) copy-start(f32[2048]{0:T(1024)} %param.28) | copy-start | bytes 24580
  108.7 38.2 %copy-start.1 = (bf16[1,2048,256]{2,1,0:T(8,128)(2,1)S(1)}, bf16[1,2048,256]{2,1,0:T(8,128)(2,1)}, u32[]{:S(2)}) copy-start(bf16[1,2048,256]{2,1,0:T(8,128)(2,1)} %param.32) | copy-start | bytes 3145732
  108.8 119.8 %reduce-scatter.2.cloned.1.call-start = ((), (), s32[]{:S(2)}) async-start(), calls=%async_computation.4 | async-start | bytes 10485760 | tf_op jit(solution)/shard_map/reduce_scatter | solution.py:156
  157.0 80.3 %copy-start.4 = (f32[64,2]{0,1:T(2,128)S(1)}, f32[64,2]{0,1:T(2,128)}, u32[]{:S(2)}) copy-start(f32[64,2]{0,1:T(2,128)} %param.30) | copy-start | bytes 1540
  231.3 29.2 %all-to-all-start.1 = ((bf16[8,32,2048]{2,1,0:T(8,128)(2,1)}), bf16[8,32,2048]{2,1,0:T(8,128)(2,1)S(1)}, u32[]{:S(2)}, u32[]{:S(2)}) async-start(bf16[8,32,2048]{2,1,0:T(8,128)(2,1)} %bitcast.117), calls=%async_computation.2 | async-start | bytes 2097152 | tf_op jit(solution)/shard_map/all_to_all | solution.py:163
Sparse Core Ops, SparseCore 0:
  14.2 40.2 all-gather.5
  108.9 33.2 all-gather.3
  157.1 71.3 reduce-scatter.1
where the time goes:
time: 278 us; the launch traced here: 274 us
  waiting for transfers between devices  141 us (51%)
  blocking collectives  61 us (22%)
  matrix products  20.9 us (8%)
  other arithmetic  20.1 us (7%)
  between operations  13.4 us (5%)
  local copies, waits for them, and re-layouts  11.3 us (4%)
  starting transfers between devices  6.31 us (2%)
    reduce_scatter x1, waiting for transfers between devices, per_device(): lax.psum_scatter(jnp.dot(hidden_flat, w_down, preferred_element_type=f32)...  71.5 us
    all_to_all x1, blocking collectives, per_device(): lax.all_to_all(outgoing, 'sp', split_axis=1, concat_axis=1, tiled=True)  35.8 us
    all_gather x1, waiting for transfers between devices, per_device(): lax.all_gather(arrived, 'tp', axis=0, tiled=True)  33.1 us
    all_to_all x1, waiting for transfers between devices, per_device(): lax.all_to_all(expert_out, 'sp', split_axis=0, concat_axis=0, tiled=True)  21.5 us
    all_gather x1, blocking collectives, entering(): gathered = jax.tree.map(lambda a: lax.all_gather(a, axis), part)  18 us
    all_gather x1, waiting for transfers between devices, entering(): gathered = jax.tree.map(lambda a: lax.all_gather(a, axis), part)  14.5 us
    dot_general x1, matrix products, per_device(): jnp.dot(hidden_flat, w_down, preferred_element_type=f32)  10 us
    all_gather x1, blocking collectives, per_device(): lax.all_gather(gated, 'tp', axis=1, tiled=True)  7.15 us
  transfers between devices with their start and end apart: 4, of which 4 were waited for; matrix products, arithmetic and copies ran while one was open for 3% of the time, Pallas kernels for 0%

commit v1 on v0

v1 whole, which is shorter than its diff:
```python
import functools

import jax
import jax.numpy as jnp
from jax import lax
from jax.experimental import pallas as pl
from jax.experimental.pallas import tpu as pltpu
from jax.sharding import PartitionSpec as P

BLOCK = 64


EPS = 1e-06
HIGH = lax.Precision.HIGHEST
MESH = pl.DeviceIdType.MESH
VMEM_LIMIT = 60 * 1024 * 1024


def xor(a, b, size):
    total, bit = 0, 1
    while bit < size:
        total = total + lax.rem(lax.div(a, jnp.int32(bit)) + lax.div(jnp.int32(b), jnp.int32(bit)), jnp.int32(2)) * bit
        bit *= 2
    return total


def loop(lo, hi, body):
    lax.fori_loop(lo, hi, lambda i, c: (body(i), c)[1], 0)


def carry_kernel(n, state_ref, decay_ref, out_ref, send, states, decays, ss, rs, ds, dr):
    s, t = lax.axis_index("sp"), lax.axis_index("tp")
    barrier = pltpu.get_barrier_semaphore()
    loop(1, n, lambda k: pl.semaphore_signal(barrier, inc=1, device_id=(lax.rem(s + k, n), t), device_id_type=MESH))
    send[...] = state_ref[...].astype(jnp.bfloat16)
    pl.semaphore_wait(barrier, n - 1)

    def copies(k, source, target):
        a = pltpu.make_async_remote_copy(
            src_ref=send, dst_ref=states.at[source], send_sem=ss.at[k], recv_sem=rs.at[k],
            device_id=(target, t), device_id_type=MESH)
        b = pltpu.make_async_remote_copy(
            src_ref=decay_ref, dst_ref=decays.at[source], send_sem=ds.at[k], recv_sem=dr.at[k],
            device_id=(target, t), device_id_type=MESH)
        return a, b

    def start(k):
        @pl.when(s + k < n)
        def _():
            for c in copies(k, s, s + k):
                c.start()

    loop(1, n, start)

    def arrive(k):
        @pl.when(s >= k)
        def _():
            for c in copies(k, s - k, s - k):
                c.wait_recv()

    loop(1, n, arrive)
    out_ref[...] = jnp.zeros_like(out_ref)

    def fold(j):
        @pl.when(j < s)
        def _():
            out_ref[...] = out_ref[...] * decays[j][:, None, :] + states[j].astype(jnp.float32)

    loop(0, n, fold)

    def sent(k):
        @pl.when(s + k < n)
        def _():
            for c in copies(k, s, s + k):
                c.wait_send()

    loop(1, n, sent)


def carry_in(n, state, decay):
    lanes, width = decay.shape
    return pl.pallas_call(
        functools.partial(carry_kernel, n),
        out_shape=jax.ShapeDtypeStruct(state.shape, jnp.float32),
        in_specs=[pl.BlockSpec(memory_space=pltpu.VMEM)] * 2,
        out_specs=pl.BlockSpec(memory_space=pltpu.VMEM),
        scratch_shapes=[
            pltpu.VMEM(state.shape, jnp.bfloat16),
            pltpu.VMEM((n,) + state.shape, jnp.bfloat16),
            pltpu.VMEM((n,) + decay.shape, jnp.float32),
        ] + [pltpu.SemaphoreType.DMA((n,))] * 4,
        compiler_params=pltpu.CompilerParams(collective_id=0, has_side_effects=True, vmem_limit_bytes=VMEM_LIMIT),
        name="carry_in",
    )(state, decay)


def expert_kernel(
    n, tps, rows, cap,
    gated_ref, stream_ref, gain_ref, place_ref, whi_ref, wlo_ref, wo_hbm, wg_hbm, wu_hbm, wd_hbm,
    out_ref,
    gbuf, wo, wg, wu, wd, mixed, normed, outgoing, arr, part, keep, keep2, rb1, sb2, rb2, back, ret,
    wsem, gs, gr, ds, dr, ys, yr, cs, cr, s1s, s1r, s2s, s2r, bs, br,
):
    f32, bf16 = jnp.float32, jnp.bfloat16
    s, t = lax.axis_index("sp"), lax.axis_index("tp")
    ty, tc = lax.div(t, jnp.int32(2)), lax.rem(t, jnp.int32(2))
    far, near = t + 2 - 4 * ty, t + 1 - 2 * tc
    mine, pair, other_pair = tc * 2 + ty, tc * 2, 2 - tc * 2
    width = stream_ref.shape[1]
    cw = gbuf.shape[2]
    loads = [pltpu.make_async_copy(a, b, wsem.at[i]) for i, (a, b) in enumerate(
        ((wo_hbm, wo), (wg_hbm, wg), (wu_hbm, wu), (wd_hbm, wd)))]
    for c in loads:
        c.start()
    barrier = pltpu.get_barrier_semaphore()
    loop(1, n, lambda k: pl.semaphore_signal(barrier, inc=1, device_id=(xor(s, k, n), t), device_id_type=MESH))
    for j in range(1, tps):
        pl.semaphore_signal(barrier, inc=1, device_id=(s, xor(t, j, tps)), device_id_type=MESH)
    pl.semaphore_wait(barrier, n - 1 + tps - 1)

    def remote(src, dst, send, recv, device):
        return pltpu.make_async_remote_copy(
            src_ref=src, dst_ref=dst, send_sem=send, recv_sem=recv, device_id=device, device_id_type=MESH)

    def g_copy(j):
        q = xor(t, j, tps)
        return remote(gated_ref.at[q], gbuf.at[t], gs.at[j], gr.at[j], (s, q))

    for j in range(1, tps):
        g_copy(j).start()
    gbuf[t] = gated_ref[t]
    loads[0].wait()
    for j in range(1, tps):
        g_copy(j).wait_recv()

    step = min(512, width)
    square = jnp.zeros((rows, 1), f32)
    for c in range(0, width, step):
        total = stream_ref[:, c:c + step].astype(f32)
        acc = jnp.zeros((rows, step), f32)
        for q in range(tps):
            acc = acc + jnp.dot(gbuf[q], wo[q * cw:(q + 1) * cw, c:c + step], preferred_element_type=f32)
        rounded = (total + acc).astype(bf16)
        mixed[:, c:c + step] = rounded
        wide = rounded.astype(f32)
        square = square + jnp.sum(wide * wide, axis=-1, keepdims=True)
    scale = lax.rsqrt(square / width + EPS)
    for c in range(0, width, step):
        normed[:, c:c + step] = (mixed[:, c:c + step].astype(f32) * scale * gain_ref[:, c:c + step]).astype(bf16)

    def d_copy(k):
        return remote(outgoing.at[k], arr.at[k, mine], ds.at[k], dr.at[k], (xor(s, k, n), t))

    def y_copy(k):
        return remote(arr.at[k, mine], arr.at[k, mine], ys.at[k], yr.at[k], (s, far))

    def c_copy(k):
        held = arr.at[k, pl.ds(pair, 2)]
        return remote(held, held, cs.at[k], cr.at[k], (s, near))

    def s1_copy(k):
        return remote(arr.at[k, pl.ds(other_pair, 2)], rb1.at[k], s1s.at[k], s1r.at[k], (s, near))

    def s2_copy(k):
        return remote(sb2.at[k], rb2.at[k], s2s.at[k], s2r.at[k], (s, far))

    def b_copy(k):
        return remote(back.at[k], ret.at[s], bs.at[k], br.at[k], (xor(s, k, n), t))

    def dispatch(k):
        block = jnp.dot(place_ref[xor(s, k, n)], normed[...], preferred_element_type=f32).astype(bf16)
        outgoing[k] = block
        d_copy(k).start()

    arr[0, mine] = jnp.dot(place_ref[s], normed[...], preferred_element_type=f32).astype(bf16)
    loop(1, n, dispatch)
    for c in loads[1:]:
        c.wait()

    def turn(i):
        @pl.when(i < n)
        def _():
            @pl.when(i > 0)
            def _():
                d_copy(i).wait_recv()
            y_copy(i).start()

        b = i - 1
        @pl.when((b >= 0) & (b < n))
        def _():
            y_copy(b).wait_recv()
            c_copy(b).start()

        e = i - 4
        @pl.when((e >= 0) & (e < n))
        def _():
            s2_copy(e).wait_recv()
            done = (keep2[lax.rem(e, jnp.int32(2))] + rb2[e].astype(f32)).astype(bf16)

            @pl.when(e == 0)
            def _():
                ret[s] = done

            @pl.when(e > 0)
            def _():
                back[e] = done
                b_copy(e).start()

        d = i - 3
        @pl.when((d >= 0) & (d < n))
        def _():
            s1_copy(d).wait_recv()
            slot = lax.rem(d, jnp.int32(2))
            sb2[d] = (keep[slot, 1 - ty] + rb1[d, 1 - ty].astype(f32)).astype(bf16)
            s2_copy(d).start()
            keep2[slot] = keep[slot, ty] + rb1[d, ty].astype(f32)

        c = i - 2
        @pl.when((c >= 0) & (c < n))
        def _():
            c_copy(c).wait_recv()
            x = arr[c].reshape(tps * cap, width)
            gate = jnp.dot(x, wg[...], preferred_element_type=f32)
            up = jnp.dot(x, wu[...], preferred_element_type=f32)
            hidden = (gate * jax.nn.sigmoid(gate) * up).astype(bf16)
            for k in range(0, width, step):
                piece = jnp.dot(hidden, wd[:, k:k + step], preferred_element_type=f32)
                part[:, :, k:k + step] = piece.reshape(tps, cap, step)
            arr[c, pl.ds(other_pair, 2)] = part[pl.ds(other_pair, 2)].astype(bf16)
            s1_copy(c).start()
            keep[lax.rem(c, jnp.int32(2))] = part[pl.ds(pair, 2)]

    loop(0, n + 4, turn)

    def arrived(k):
        b_copy(k).wait_recv()

    loop(1, n, arrived)
    for c in range(0, width, step):
        held = ret[:, :, c:c + step].reshape(n * cap, step)
        routed = jnp.dot(whi_ref[...], held, preferred_element_type=f32)
        routed = routed + jnp.dot(wlo_ref[...], held, preferred_element_type=f32)
        out_ref[:, c:c + step] = (mixed[:, c:c + step].astype(f32) + routed).astype(bf16)

    for j in range(1, tps):
        g_copy(j).wait_send()

    def sent(k):
        y_copy(k).wait_send()
        c_copy(k).wait_send()
        s1_copy(k).wait_send()
        s2_copy(k).wait_send()

        @pl.when(k > 0)
        def _():
            d_copy(k).wait_send()
            b_copy(k).wait_send()

    loop(0, n, sent)


def experts_of(n, tps, cap, gated, stream, gain, place, whi, wlo, w_out, w_gate, w_up, w_down):
    rows, width = stream.shape
    bf16, f32 = jnp.bfloat16, jnp.float32
    vmem = pl.BlockSpec(memory_space=pltpu.VMEM)
    hbm = pl.BlockSpec(memory_space=pl.ANY)
    block = (cap, width)
    sem = pltpu.SemaphoreType.DMA
    return pl.pallas_call(
        functools.partial(expert_kernel, n, tps, rows, cap),
        out_shape=jax.ShapeDtypeStruct((rows, width), bf16),
        in_specs=[vmem] * 6 + [hbm] * 4,
        out_specs=vmem,
        scratch_shapes=[
            pltpu.VMEM(gated.shape, bf16),
            pltpu.VMEM(w_out.shape, bf16),
            pltpu.VMEM(w_gate.shape, bf16),
            pltpu.VMEM(w_up.shape, bf16),
            pltpu.VMEM(w_down.shape, bf16),
            pltpu.VMEM((rows, width), bf16),
            pltpu.VMEM((rows, width), bf16),
            pltpu.VMEM((n,) + block, bf16),
            pltpu.VMEM((n, tps) + block, bf16),
            pltpu.VMEM((tps,) + block, f32),
            pltpu.VMEM((2, 2) + block, f32),
            pltpu.VMEM((2,) + block, f32),
            pltpu.VMEM((n, 2) + block, bf16),
            pltpu.VMEM((n,) + block, bf16),
            pltpu.VMEM((n,) + block, bf16),
            pltpu.VMEM((n,) + block, bf16),
            pltpu.VMEM((n,) + block, bf16),
            sem((4,)), sem((tps,)), sem((tps,)),
        ] + [sem((n,))] * 12,
        compiler_params=pltpu.CompilerParams(collective_id=1, has_side_effects=True, vmem_limit_bytes=VMEM_LIMIT),
        name="experts",
    )(gated, stream, gain, place, whi, wlo, w_out, w_gate, w_up, w_down)


def cut_to_segments(array, segment_span, heads):
    width = array.shape[1] // heads
    shaped = array.astype(jnp.float32).reshape(
        array.shape[0] // segment_span, segment_span, heads, width
    )
    return jnp.transpose(shaped, (0, 2, 1, 3))


def slot_ranks(chosen, experts):
    onehot = (chosen[:, :, None] == jnp.arange(experts, dtype=jnp.int32)[None, None, :]).astype(
        jnp.int32
    )
    earlier = jnp.cumsum(onehot, axis=1) - onehot
    return jnp.sum(earlier * onehot, axis=2)


def per_device(
    stream,
    query,
    forget_gate_logits,
    value_input_rows,
    output_gate_logits,
    forget_floor_margin,
    additional_fading_speed,
    head_norm_gain,
    output_head_weight,
    feedforward_norm_gain,
    selected_expert_index,
    selected_expert_weight,
    expert_gate_weight,
    expert_up_weight,
    expert_down_weight,
):
    f32 = jnp.float32
    tok_rows, model_width = stream.shape
    local_scan_lanes, head_dim = forget_floor_margin.shape
    segment_span = BLOCK
    tp_count = lax.axis_size("tp")
    tp_rank = lax.axis_index("tp")
    query_blk = cut_to_segments(query, segment_span, local_scan_lanes)
    scores_segment_slice = cut_to_segments(forget_gate_logits, segment_span, local_scan_lanes)
    value_blk = cut_to_segments(value_input_rows, segment_span, local_scan_lanes)
    spike_segment_slice = cut_to_segments(additional_fading_speed, segment_span, local_scan_lanes)
    clearance_amount = forget_floor_margin[None, :, None, :]
    logarithmic_fading_speed = (
        jnp.logaddexp(
            jnp.log1p(-clearance_amount),
            jnp.log(clearance_amount) + jax.nn.log_sigmoid(scores_segment_slice),
        )
        + spike_segment_slice
    )
    key_in = clearance_amount * jax.nn.sigmoid(-scores_segment_slice)
    cumul = jnp.cumsum(logarithmic_fading_speed, axis=2)
    last = cumul[:, :, -1:, :]
    causal = jnp.tril(jnp.ones((segment_span, segment_span), dtype=bool))[:, :, None]
    pair_log = cumul[:, :, :, None, :] - cumul[:, :, None, :, :]
    decay = jnp.exp(jnp.where(causal, pair_log, -jnp.inf))
    scores = jnp.sum(query_blk[:, :, :, None, :] * key_in[:, :, None, :, :] * decay, axis=-1)
    inner = jnp.einsum("bhts,bhse->bhte", scores, value_blk, precision=HIGH)
    block_state = jnp.einsum(
        "bhsd,bhse->bhed", key_in * jnp.exp(last - cumul), value_blk, precision=HIGH
    )
    block_last = last[:, :, 0, :]
    last_cumul = jnp.cumsum(block_last, axis=0)
    device_decay = jnp.exp(last_cumul[-1])
    suffix = jnp.exp(last_cumul[-1][None] - last_cumul)
    local_final = jnp.sum(suffix[:, :, None, :] * block_state, axis=0)
    n = lax.axis_size("sp")
    incoming = carry_in(n, local_final, device_decay)
    chain_starts = []
    for blk in range(block_state.shape[0]):
        chain_starts.append(incoming)
        incoming = jnp.exp(block_last[blk])[:, None, :] * incoming + block_state[blk]
    recur = inner + jnp.einsum(
        "bhtd,bhed->bhte", query_blk * jnp.exp(cumul), jnp.stack(chain_starts), precision=HIGH
    )
    recur = jnp.transpose(recur, (0, 2, 1, 3)).reshape(tok_rows, local_scan_lanes, head_dim)
    scale = lax.rsqrt(jnp.mean(recur * recur, axis=-1, keepdims=True) + EPS)
    gate_in = output_gate_logits.astype(f32).reshape(tok_rows, local_scan_lanes, head_dim)
    gated = (
        (recur * scale * head_norm_gain * jax.nn.silu(gate_in))
        .astype(jnp.bfloat16)
        .reshape(tok_rows, local_scan_lanes * head_dim)
    )
    topk = selected_expert_index.shape[1]
    experts = n * expert_gate_weight.shape[0]
    group_rows = tok_rows // tp_count
    cap = 2 * topk * group_rows // experts
    cap = -(-cap // 16) * 16
    own_route = lax.dynamic_slice_in_dim(selected_expert_index, tp_rank * group_rows, group_rows, 0)
    own_stream = lax.dynamic_slice_in_dim(stream, tp_rank * group_rows, group_rows, 0)
    own_ranks = slot_ranks(own_route.reshape(1, -1), experts)[0].reshape(group_rows, topk)
    slot = own_route * cap + own_ranks
    slots = jnp.arange(experts * cap, dtype=jnp.int32)
    place = jnp.zeros((experts * cap, group_rows), f32)
    weight = jnp.zeros((group_rows, experts * cap), f32)
    for j in range(topk):
        place = place + (slot[:, j][None, :] == slots[:, None]).astype(f32)
        weight = weight + jnp.where(
            slot[:, j][:, None] == slots[None, :], selected_expert_weight[:, j][:, None], 0.0
        )
    place = place.astype(jnp.bfloat16).reshape(experts, cap, group_rows)
    weight_high = lax.reduce_precision(weight, 8, 7)
    weight_low = (weight - weight_high).astype(jnp.bfloat16)
    return experts_of(
        n,
        tp_count,
        cap,
        gated.reshape(tp_count, group_rows, local_scan_lanes * head_dim),
        own_stream,
        feedforward_norm_gain[None, :],
        place,
        weight_high.astype(jnp.bfloat16),
        weight_low,
        output_head_weight,
        expert_gate_weight[0],
        expert_up_weight[0],
        expert_down_weight[0],
    )


def solution(mesh):
    return jax.shard_map(
        per_device,
        mesh=mesh,
        in_specs=(
            P("sp", None),
            P("sp", "tp"),
            P("sp", "tp"),
            P("sp", "tp"),
            P("sp", "tp"),
            P("tp", None),
            P("sp", "tp"),
            P(),
            P(),
            P(),
            P("sp", None),
            P(("sp", "tp"), None),
            P("sp", None, "tp"),
            P("sp", None, "tp"),
            P("sp", "tp", None),
        ),
        out_specs=P(("sp", "tp"), None),
        check_vma=False,
    )
```

time: 278 us -> 116 us (0.42); the launches traced: 274 us -> 116 us
  waiting for transfers between devices: 141 us -> 0 us
  Pallas kernels: 0 us -> 93.7 us
  blocking collectives: 61 us -> 0 us
  matrix products: 20.9 us -> 3.46 us
  between operations: 13.4 us -> 0.26 us
  other arithmetic: 20.1 us -> 12.2 us
  starting transfers between devices: 6.31 us -> 0 us
  local copies, waits for them, and re-layouts: 11.3 us -> 6.44 us
    pallas_call x0 -> x2, Pallas kernels: none -> 93.7 us  [the longest x1 77 us: experts_of(): pl.pallas_call(functools.partial(expert_kernel, n, tps, rows, cap), out_s...]
    reduce_scatter x1 -> x0, waiting for transfers between devices: 71.5 us -> none  [per_device(): lax.psum_scatter(jnp.dot(hidden_flat, w_down, preferred_element_type=f32)...]
    all_gather x2 -> x0, waiting for transfers between devices: 47.6 us -> none  [the longest x1 33.1 us: per_device(): lax.all_gather(arrived, 'tp', axis=0, tiled=True)]
    all_to_all x1 -> x0, blocking collectives: 35.8 us -> none  [per_device(): lax.all_to_all(outgoing, 'sp', split_axis=1, concat_axis=1, tiled=True)]
    all_gather x2 -> x0, blocking collectives: 25.2 us -> none  [the longest x1 18 us: entering(): gathered = jax.tree.map(lambda a: lax.all_gather(a, axis), part)]
    all_to_all x1 -> x0, waiting for transfers between devices: 21.5 us -> none  [per_device(): lax.all_to_all(expert_out, 'sp', split_axis=0, concat_axis=0, tiled=True)]
    dot_general x5 -> x2, matrix products: 20.6 us -> 3.2 us  [the longest x1 2.12 us: per_device(): jnp.einsum('bhtd,bhed->bhte', query_blk * jnp.exp(cumul), jnp.stack(chain...]
    all_to_all x1 -> x0, starting transfers between devices: 6.04 us -> none  [per_device(): lax.all_to_all(expert_out, 'sp', split_axis=0, concat_axis=0, tiled=True)]
  transfers between devices with their start and end apart: 4 -> 0, of which waited for: 4 -> 0; matrix products, arithmetic and copies ran while one was open for 3% -> 0% of each run, Pallas kernels for 0% -> 0%
where the time goes in v1:
time: 116 us
  Pallas kernels  93.7 us (81%)
  other arithmetic  12.2 us (11%)
  local copies, waits for them, and re-layouts  6.44 us (6%)
  matrix products  3.46 us (3%)
    pallas_call x1, Pallas kernels, experts_of(): pl.pallas_call(functools.partial(expert_kernel, n, tps, rows, cap), out_s...  77 us
    pallas_call x1, Pallas kernels, carry_in(): pl.pallas_call(functools.partial(carry_kernel, n), out_shape=jax.ShapeDty...  16.7 us
    reduce_sum x1, other arithmetic, per_device(): jnp.sum(query_blk[:, :, :, None, :] * key_in[:, :, None, :, :] * decay, a...  5.5 us

profile of v1, /device:TPU:8, one launch (start us, length us, event | category | flops | bytes accessed | tf_op | source)
XLA Modules:
  0.0 116.1 jit_solution(8527009227108093799)
XLA Ops:
  0.0 0.0 copy-start
  0.0 1.1 fusion.8
  1.1 0.1 neg.35
  1.2 0.8 reshape.205
  2.0 0.7 negate_log-plus-one_fusion
  2.7 0.3 select_add_fusion
  3.0 0.2 reduce_window_sum.33
  3.3 0.1 div.19
  3.4 1.0 reshape.212
  4.4 0.7 fusion.21
  5.2 0.0 copy-start.1
  5.2 5.5 %multiply_reduce_fusion = f32[4,2,64,64]{3,2,1,0:T(8,128)S(1)} fusion(f32[4,2,64,128]{3,2,1,0:T(8,128)S(1)} %reduce_window_sum.33, f32[4,2,64,128]{3,2,1,0:T(8,128)S(1)} %get-tuple-element.25, f32[4,2,64,128]{3,2,1,0:T(8,128)S(1)} %get-tuple-element.26, pred[64,64]{1,0:T(8,128)(4,1)S(1)} %iota_compare_fusion.3), kind=kLoop, calls=%fused_computation | loop fusion | flops 20938752 | bytes 921600 | tf_op jit(solution)/shard_map/reduce_sum | solution.py:356
  10.7 0.0 copy-done.1
  10.7 0.0 copy-start.5
  10.7 0.0 copy-start.2
  10.7 0.0 copy-start.4
  10.8 0.0 copy-start.3
  10.8 0.3 fusion.33
  11.1 1.1 multiply_reduce_fusion.1
  12.2 0.6 fusion.44.decay_ref
  12.8 16.7 %carry_in.1 = f32[2,128,128]{2,1,0:T(8,128)} custom-call(f32[2,128,128]{2,1,0:T(8,128)} %get-tuple-element.21.state_ref, f32[2,128]{1,0:T(2,128)} %fusion.44.decay_ref), custom_call_target="tpu_custom_call" | custom-call | tf_op jit(solution)/shard_map/carry_in/pallas_call | solution.py:82
  29.5 0.9 fusion.29
  30.5 2.1 %fusion.16 = (f32[4,64,2]{1,2,0:T(2,128)S(1)}, f32[4,2,64,128]{3,2,1,0:T(8,128)S(1)}) fusion(f32[4,2,64,128]{3,2,1,0:T(8,128)S(1)} %fusion.33, f32[1,2,128,128]{3,2,1,0:T(8,128)S(1)} %get-tuple-element.7, f32[1,2,128,128]{3,2,1,0:T(8,128)S(1)} %bitcast.115, f32[1,2,128,128]{3,2,1,0:T(8,128)S(1)} %get-tuple-element.9, f32[1,2,128,128]{3,2,1,0:T(8,128)} %bitcast.110, ...), kind=kOutput, calls=%fused_computation.27 | convolution fusion | flops 101318144 | bytes 1574912 | tf_op jit(solution)/shard_map/bhtd,bhed->bhte/dot_general | solution.py:372
  32.6 0.1 copy.75
  32.7 0.3 mul.133
  33.1 0.2 mul.134
  33.3 0.0 copy-done.5
  33.3 0.0 copy-done.2
  33.3 0.8 fusion.27.gated_ref
  34.1 0.0 copy-done
  34.1 0.7 constant_dynamic-slice_fusion.1.stream_ref
  34.8 0.0 copy-done.4
  34.8 0.1 constant_dynamic-slice_fusion
  34.9 0.1 copy.77
  35.0 0.1 eq.95
  35.1 0.1 fusion.39
  35.2 0.2 reduce_window_sum.35
  35.4 0.2 select_reduce_fusion
  35.6 0.1 reshape_squeeze.3
  35.7 0.2 slice_reduce_fusion.1
  35.9 0.7 add_convert_fusion.place_ref
  36.6 0.0 copy-done.3
  36.7 0.7 fusion.38
  37.4 77.0 %experts.1 = bf16[64,2048]{1,0:T(8,128)(2,1)} custom-call(bf16[4,64,256]{2,1,0:T(8,128)(2,1)} %fusion.27.gated_ref, bf16[64,2048]{1,0:T(8,128)(2,1)} %constant_dynamic-slice_fusion.1.stream_ref, f32[1,2048]{1,0:T(1,128)} %bitcast.123, bf16[8,32,64]{2,1,0:T(8,128)(2,1)} %add_convert_fusion.place_ref, bf16[64,256]{1,0:T(8,128)(2,1)} %get-tuple-element.16.whi_ref, ...), custom_call_target="tpu_custom_call" | custom-call | tf_op jit(solution)/shard_map/experts/pallas_call | solution.py:269
  114.4 1.7 %copy.110 = bf16[64,2048]{1,0:T(8,128)(2,1)} copy(bf16[64,2048]{1,0:T(8,128)(2,1)} %experts.1) | data formatting | bytes 524288
  (14 shorter events, 0.1 us)
Async XLA Ops:
  0.0 34.1 %copy-start = (bf16[256,2048]{1,0:T(8,128)(2,1)S(1)}, bf16[256,2048]{1,0:T(8,128)(2,1)}, u32[]{:S(2)}) copy-start(bf16[256,2048]{1,0:T(8,128)(2,1)} %param.15) | copy-start | bytes 3145732
  5.2 5.5 %copy-start.1 = (bf16[256,256]{1,0:T(8,128)(2,1)S(1)}, bf16[256,256]{1,0:T(8,128)(2,1)}, u32[]{:S(2)}) copy-start(bf16[256,256]{1,0:T(8,128)(2,1)} %param.18) | copy-start | bytes 393220
  10.7 22.6 %copy-start.5 = (f32[128]{0:T(128)S(1)}, f32[128]{0:T(128)}, u32[]{:S(2)}) copy-start(f32[128]{0:T(128)} %param.22) | copy-start | bytes 1540
  10.7 22.6 %copy-start.2 = (bf16[256,256]{1,0:T(8,128)(2,1)S(1)}, bf16[256,256]{1,0:T(8,128)(2,1)}, u32[]{:S(2)}) copy-start(bf16[256,256]{1,0:T(8,128)(2,1)} %param.19) | copy-start | bytes 393220
  10.7 24.1 %copy-start.4 = (s32[256,2]{0,1:T(2,128)S(1)}, s32[256,2]{0,1:T(2,128)}, u32[]{:S(2)}) copy-start(s32[256,2]{0,1:T(2,128)} %param.25) | copy-start | bytes 6148
  10.8 25.9 %copy-start.3 = (f32[64,2]{0,1:T(2,128)S(1)}, f32[64,2]{0,1:T(2,128)}, u32[]{:S(2)}) copy-start(f32[64,2]{0,1:T(2,128)} %param.26) | copy-start | bytes 1540

commit v2 on v1

--- a/solution.py
+++ b/solution.py
@@ -8,6 +8,7 @@
 from jax.sharding import PartitionSpec as P
 
 BLOCK = 64
+SUB = 16
 
 
 EPS = 1e-06
@@ -28,11 +29,39 @@
     lax.fori_loop(lo, hi, lambda i, c: (body(i), c)[1], 0)
 
 
-def carry_kernel(n, state_ref, decay_ref, out_ref, send, states, decays, ss, rs, ds, dr):
+def wide_dot(a, b, contract):
+    return lax.dot_general(a, b, ((contract[:1], contract[1:]), ((), ())), precision=HIGH, preferred_element_type=jnp.float32)
+
+
+def scan_kernel(
+    n, lanes, dim, query_ref, logit_ref, value_ref, gate_ref, margin_ref, fade_ref, gain_ref, out_ref,
+    cum, key, rec, chain, send, decay, carried, states, decays, ss, rs, ds, dr,
+):
+    f32, bf16 = jnp.float32, jnp.bfloat16
     s, t = lax.axis_index("sp"), lax.axis_index("tp")
+    rows = query_ref.shape[0]
+    count = rows // BLOCK
     barrier = pltpu.get_barrier_semaphore()
     loop(1, n, lambda k: pl.semaphore_signal(barrier, inc=1, device_id=(lax.rem(s + k, n), t), device_id_type=MESH))
-    send[...] = state_ref[...].astype(jnp.bfloat16)
+    heads = [slice(h * dim, (h + 1) * dim) for h in range(lanes)]
+    row = lax.broadcasted_iota(jnp.int32, (BLOCK, BLOCK), 0)
+    lower = (row >= lax.broadcasted_iota(jnp.int32, (BLOCK, BLOCK), 1)).astype(f32)
+    for h, sl in enumerate(heads):
+        entering_key = margin_ref[h:h + 1, :] * jax.nn.sigmoid(-logit_ref[:, sl].astype(f32))
+        key[:, sl] = entering_key
+        rec[:, sl] = jnp.log1p(-entering_key) + fade_ref[:, h:h + 1]
+    for b in range(count):
+        part = slice(b * BLOCK, (b + 1) * BLOCK)
+        cum[part, :] = wide_dot(lower, rec[part, :], (1, 0))
+    offsets = [jnp.zeros((1, lanes * dim), f32)]
+    for b in range(count):
+        offsets.append(offsets[-1] + cum[(b + 1) * BLOCK - 1:(b + 1) * BLOCK, :])
+    for b in range(count):
+        part = slice(b * BLOCK, (b + 1) * BLOCK)
+        rec[part, :] = key[part, :] * jnp.exp(offsets[-1] - offsets[b] - cum[part, :])
+    for h, sl in enumerate(heads):
+        send[h] = wide_dot(value_ref[:, sl].astype(f32), rec[:, sl], (0, 0)).astype(bf16)
+        decay[h:h + 1, :] = jnp.exp(offsets[-1][:, sl])
     pl.semaphore_wait(barrier, n - 1)
 
     def copies(k, source, target):
@@ -40,7 +69,7 @@
             src_ref=send, dst_ref=states.at[source], send_sem=ss.at[k], recv_sem=rs.at[k],
             device_id=(target, t), device_id_type=MESH)
         b = pltpu.make_async_remote_copy(
-            src_ref=decay_ref, dst_ref=decays.at[source], send_sem=ds.at[k], recv_sem=dr.at[k],
+            src_ref=decay, dst_ref=decays.at[source], send_sem=ds.at[k], recv_sem=dr.at[k],
             device_id=(target, t), device_id_type=MESH)
         return a, b
 
@@ -51,6 +80,36 @@
                 c.start()
 
     loop(1, n, start)
+    chain[...] = jnp.zeros_like(chain)
+    near = lax.broadcasted_iota(jnp.int32, (BLOCK // SUB, SUB, 1), 1)
+    below = lax.broadcasted_iota(jnp.int32, (BLOCK, 1), 0)
+
+    def inside(b):
+        part = pl.ds(pl.multiple_of(b * BLOCK, BLOCK), BLOCK)
+        for h, sl in enumerate(heads):
+            q, v = query_ref[part, sl].astype(f32), value_ref[part, sl].astype(f32)
+            c, k = cum[part, sl], key[part, sl]
+            cut = (BLOCK // SUB, SUB, dim)
+            q3, v3, c3, k3 = q.reshape(cut), v.reshape(cut), c.reshape(cut), k.reshape(cut)
+            inner = jnp.zeros(cut, f32)
+            for j in range(SUB):
+                fade = jnp.exp(jnp.minimum(c3 - c3[:, j:j + 1, :], 0.0))
+                score = jnp.sum(q3 * fade * k3[:, j:j + 1, :], axis=-1, keepdims=True)
+                inner = inner + jnp.where(near >= j, score, 0.0) * v3[:, j:j + 1, :]
+            scores = [jnp.zeros((SUB, BLOCK), f32)]
+            for i in range(SUB, BLOCK, SUB):
+                edge = c[i - 1:i, :]
+                older = jnp.where(below < i, k * jnp.exp(jnp.minimum(edge - c, 0.0)), 0.0)
+                scores.append(wide_dot(q[i:i + SUB] * jnp.exp(c[i:i + SUB] - edge), older, (1, 1)))
+            last = c[BLOCK - 1:BLOCK, :]
+            rec[part, sl] = (
+                inner.reshape(BLOCK, dim)
+                + wide_dot(jnp.concatenate(scores, axis=0), v, (1, 0))
+                + wide_dot(q * jnp.exp(c), chain[h], (1, 1))
+            )
+            chain[h] = jnp.exp(last) * chain[h] + wide_dot(v, k * jnp.exp(last - c), (0, 0))
+
+    loop(0, count, inside)
 
     def arrive(k):
         @pl.when(s >= k)
@@ -59,14 +118,23 @@
                 c.wait_recv()
 
     loop(1, n, arrive)
-    out_ref[...] = jnp.zeros_like(out_ref)
+    carried[...] = jnp.zeros_like(carried)
 
     def fold(j):
         @pl.when(j < s)
         def _():
-            out_ref[...] = out_ref[...] * decays[j][:, None, :] + states[j].astype(jnp.float32)
+            for h in range(lanes):
+                carried[h] = carried[h] * decays[j, h:h + 1, :] + states[j, h].astype(f32)
 
     loop(0, n, fold)
+    for b in range(count):
+        part = slice(b * BLOCK, (b + 1) * BLOCK)
+        cum[part, :] = jnp.exp(cum[part, :] + offsets[b])
+    for h, sl in enumerate(heads):
+        recur = rec[:, sl] + wide_dot(query_ref[:, sl].astype(f32) * cum[:, sl], carried[h], (1, 1))
+        scale = lax.rsqrt(jnp.mean(recur * recur, axis=-1, keepdims=True) + EPS)
+        gate = gate_ref[:, sl].astype(f32)
+        out_ref[:, sl] = (recur * scale * gain_ref[...] * (gate * jax.nn.sigmoid(gate))).astype(bf16)
 
     def sent(k):
         @pl.when(s + k < n)
@@ -77,21 +145,29 @@
     loop(1, n, sent)
 
 
-def carry_in(n, state, decay):
-    lanes, width = decay.shape
+def gated_scan(n, query, logits, value, gate, margin, fade, gain):
+    lanes, dim = margin.shape
+    f32, bf16 = jnp.float32, jnp.bfloat16
+    state = (lanes, dim, dim)
     return pl.pallas_call(
-        functools.partial(carry_kernel, n),
-        out_shape=jax.ShapeDtypeStruct(state.shape, jnp.float32),
-        in_specs=[pl.BlockSpec(memory_space=pltpu.VMEM)] * 2,
+        functools.partial(scan_kernel, n, lanes, dim),
+        out_shape=jax.ShapeDtypeStruct(query.shape, bf16),
+        in_specs=[pl.BlockSpec(memory_space=pltpu.VMEM)] * 7,
         out_specs=pl.BlockSpec(memory_space=pltpu.VMEM),
         scratch_shapes=[
-            pltpu.VMEM(state.shape, jnp.bfloat16),
-            pltpu.VMEM((n,) + state.shape, jnp.bfloat16),
-            pltpu.VMEM((n,) + decay.shape, jnp.float32),
+            pltpu.VMEM(query.shape, f32),
+            pltpu.VMEM(query.shape, f32),
+            pltpu.VMEM(query.shape, f32),
+            pltpu.VMEM(state, f32),
+            pltpu.VMEM(state, bf16),
+            pltpu.VMEM((lanes, dim), f32),
+            pltpu.VMEM(state, f32),
+            pltpu.VMEM((n,) + state, bf16),
+            pltpu.VMEM((n, lanes, dim), f32),
         ] + [pltpu.SemaphoreType.DMA((n,))] * 4,
         compiler_params=pltpu.CompilerParams(collective_id=0, has_side_effects=True, vmem_limit_bytes=VMEM_LIMIT),
-        name="carry_in",
-    )(state, decay)
+        name="gated_scan",
+    )(query, logits, value, gate, margin, fade, gain)
 
 
 def expert_kernel(
@@ -296,14 +372,6 @@
     )(gated, stream, gain, place, whi, wlo, w_out, w_gate, w_up, w_down)
 
 
-def cut_to_segments(array, segment_span, heads):
-    width = array.shape[1] // heads
-    shaped = array.astype(jnp.float32).reshape(
-        array.shape[0] // segment_span, segment_span, heads, width
-    )
-    return jnp.transpose(shaped, (0, 2, 1, 3))
-
-
 def slot_ranks(chosen, experts):
     onehot = (chosen[:, :, None] == jnp.arange(experts, dtype=jnp.int32)[None, None, :]).astype(
         jnp.int32
@@ -332,53 +400,18 @@
     f32 = jnp.float32
     tok_rows, model_width = stream.shape
     local_scan_lanes, head_dim = forget_floor_margin.shape
-    segment_span = BLOCK
+    n = lax.axis_size("sp")
     tp_count = lax.axis_size("tp")
     tp_rank = lax.axis_index("tp")
-    query_blk = cut_to_segments(query, segment_span, local_scan_lanes)
-    scores_segment_slice = cut_to_segments(forget_gate_logits, segment_span, local_scan_lanes)
-    value_blk = cut_to_segments(value_input_rows, segment_span, local_scan_lanes)
-    spike_segment_slice = cut_to_segments(additional_fading_speed, segment_span, local_scan_lanes)
-    clearance_amount = forget_floor_margin[None, :, None, :]
-    logarithmic_fading_speed = (
-        jnp.logaddexp(
-            jnp.log1p(-clearance_amount),
-            jnp.log(clearance_amount) + jax.nn.log_sigmoid(scores_segment_slice),
-        )
-        + spike_segment_slice
-    )
-    key_in = clearance_amount * jax.nn.sigmoid(-scores_segment_slice)
-    cumul = jnp.cumsum(logarithmic_fading_speed, axis=2)
-    last = cumul[:, :, -1:, :]
-    causal = jnp.tril(jnp.ones((segment_span, segment_span), dtype=bool))[:, :, None]
-    pair_log = cumul[:, :, :, None, :] - cumul[:, :, None, :, :]
-    decay = jnp.exp(jnp.where(causal, pair_log, -jnp.inf))
-    scores = jnp.sum(query_blk[:, :, :, None, :] * key_in[:, :, None, :, :] * decay, axis=-1)
-    inner = jnp.einsum("bhts,bhse->bhte", scores, value_blk, precision=HIGH)
-    block_state = jnp.einsum(
-        "bhsd,bhse->bhed", key_in * jnp.exp(last - cumul), value_blk, precision=HIGH
-    )
-    block_last = last[:, :, 0, :]
-    last_cumul = jnp.cumsum(block_last, axis=0)
-    device_decay = jnp.exp(last_cumul[-1])
-    suffix = jnp.exp(last_cumul[-1][None] - last_cumul)
-    local_final = jnp.sum(suffix[:, :, None, :] * block_state, axis=0)
-    n = lax.axis_size("sp")
-    incoming = carry_in(n, local_final, device_decay)
-    chain_starts = []
-    for blk in range(block_state.shape[0]):
-        chain_starts.append(incoming)
-        incoming = jnp.exp(block_last[blk])[:, None, :] * incoming + block_state[blk]
-    recur = inner + jnp.einsum(
-        "bhtd,bhed->bhte", query_blk * jnp.exp(cumul), jnp.stack(chain_starts), precision=HIGH
-    )
-    recur = jnp.transpose(recur, (0, 2, 1, 3)).reshape(tok_rows, local_scan_lanes, head_dim)
-    scale = lax.rsqrt(jnp.mean(recur * recur, axis=-1, keepdims=True) + EPS)
-    gate_in = output_gate_logits.astype(f32).reshape(tok_rows, local_scan_lanes, head_dim)
-    gated = (
-        (recur * scale * head_norm_gain * jax.nn.silu(gate_in))
-        .astype(jnp.bfloat16)
-        .reshape(tok_rows, local_scan_lanes * head_dim)
+    gated = gated_scan(
+        n,
+        query,
+        forget_gate_logits,
+        value_input_rows,
+        output_gate_logits,
+        forget_floor_margin,
+        additional_fading_speed,
+        head_norm_gain[None, :],
     )
     topk = selected_expert_index.shape[1]
     experts = n * expert_gate_weight.shape[0]

time: 116 us -> 103 us (0.89)
  other arithmetic: 12.2 us -> 1.9 us
  matrix products: 3.46 us -> 0 us
    reduce_sum x1 -> x0, other arithmetic: 5.5 us -> none  [per_device(): jnp.sum(query_blk[:, :, :, None, :] * key_in[:, :, None, :, :] * decay, a...]
    dot_general x3 -> x0, matrix products: 3.46 us -> none  [the longest x1 2.12 us: per_device(): jnp.einsum('bhtd,bhed->bhte', query_blk * jnp.exp(cumul), jnp.stack(chain...]
    unnamed x15 -> x5, local copies, waits for them, and re-layouts: 1.81 us -> 3.24 us
    another operation x3 -> x0, other arithmetic: 1.2 us -> none  [the longest x1 0.94 us: per_device(): jnp.stack(chain_starts)]
where the time goes in v2:
time: 103 us
  Pallas kernels  94.5 us (92%)
  local copies, waits for them, and re-layouts  6.02 us (6%)
  other arithmetic  1.9 us (2%)
    pallas_call x1, Pallas kernels, experts_of(): pl.pallas_call(functools.partial(expert_kernel, n, tps, rows, cap), out_s...  77.5 us
    pallas_call x1, Pallas kernels, gated_scan(): pl.pallas_call(functools.partial(scan_kernel, n, lanes, dim), out_shape=j...  17 us
    unnamed x5, local copies, waits for them, and re-layouts  3.24 us

profile of v2, /device:TPU:8, one launch (start us, length us, event | category | flops | bytes accessed | tf_op | source)
XLA Modules:
  0.0 102.5 jit_solution(18234626344918742194)
XLA Ops:
  0.0 0.0 copy-start
  0.0 0.8 constant_dynamic-slice_fusion
  0.8 0.8 slice_bitcast_fusion.1
  1.6 0.1 copy.20
  1.7 0.1 eq.95
  1.8 0.1 fusion.1
  1.9 0.2 reduce_window_sum.11
  2.1 0.2 select_reduce_fusion
  2.3 0.1 reshape_squeeze.3
  2.4 0.2 slice_reduce_fusion.1
  2.6 0.7 add_convert_fusion.place_ref
  3.4 0.7 fusion
  4.1 1.5 %copy.18.fade_ref = f32[256,2]{1,0:T(8,128)} copy(f32[256,2]{0,1:T(2,128)} %param.21) | data formatting | bytes 4096 | tf_op args[6]
  5.6 17.0 %gated_scan.1 = bf16[256,256]{1,0:T(8,128)(2,1)} custom-call(bf16[256,256]{1,0:T(8,128)(2,1)} %query_ref.1, bf16[256,256]{1,0:T(8,128)(2,1)} %logit_ref.1, bf16[256,256]{1,0:T(8,128)(2,1)} %value_ref.1, bf16[256,256]{1,0:T(8,128)(2,1)} %gate_ref.1, f32[2,128]{1,0:T(2,128)} %margin_ref.1, f32[256,2]{1,0:T(8,128)} %copy.18.fade_ref, f32[1,128]{1,0:T(1,128)} %bitcast.15), custom_call_target="tpu_custom_call" | custom-call | tf_op jit(solution)/shard_map/gated_scan/pallas_call | solution.py:152
  22.6 0.0 copy-done
  22.6 0.7 constant_dynamic-slice_fusion.1.stream_ref
  23.3 77.5 %experts.1 = bf16[64,2048]{1,0:T(8,128)(2,1)} custom-call(bf16[4,64,256]{2,1,0:T(8,128)(2,1)} %bitcast.13, bf16[64,2048]{1,0:T(8,128)(2,1)} %constant_dynamic-slice_fusion.1.stream_ref, f32[1,2048]{1,0:T(1,128)} %bitcast.14, bf16[8,32,64]{2,1,0:T(8,128)(2,1)} %add_convert_fusion.place_ref, bf16[64,256]{1,0:T(8,128)(2,1)} %get-tuple-element.8.whi_ref, ...), custom_call_target="tpu_custom_call" | custom-call | tf_op jit(solution)/shard_map/experts/pallas_call | solution.py:345
  100.8 1.7 %copy.22 = bf16[64,2048]{1,0:T(8,128)(2,1)} copy(bf16[64,2048]{1,0:T(8,128)(2,1)} %experts.1) | data formatting | bytes 524288
  (2 shorter events, 0.0 us)
Async XLA Ops:
  0.0 22.6 %copy-start = (bf16[256,2048]{1,0:T(8,128)(2,1)S(1)}, bf16[256,2048]{1,0:T(8,128)(2,1)}, u32[]{:S(2)}) copy-start(bf16[256,2048]{1,0:T(8,128)(2,1)} %param.15) | copy-start | bytes 3145732
